TPU v7x, 32 devices: a whole 2x2x4 slice. The times are simulated.
32 devices in a mesh: grp: 2 (over y), sp: 4 (over z), tp: 4 (over x, core).
Axes of the slice: x: 2, y: 2, z: 4, core: 2. Of those that a mesh axis runs over, the one named last changes fastest.
Arguments:
- tokens: bfloat16 [1024, 2048], P(('grp', 'sp')), parts along dimension 0, may hold values from -6 to 6
- norm_gain: float32 [2048], replicated, may hold values from 0.1 to 1.9
- w_query: bfloat16 [2048, 512], P('sp', 'tp'), may hold values from -0.125 to 0.125
- w_key: bfloat16 [2048, 512], P('sp', 'tp'), may hold values from -0.125 to 0.125
- w_value: bfloat16 [2048, 512], P('sp', 'tp'), may hold values from -0.125 to 0.125
- w_glu_value: bfloat16 [2048, 1024], P('sp', 'tp'), may hold values from -0.125 to 0.125
- w_glu_gate: bfloat16 [2048, 1024], P('sp', 'tp'), may hold values from -0.125 to 0.125
- key_offset: bfloat16 [1024, 8], P(('grp', 'sp'), 'tp'), parts along dimension 0, may hold values from -13 to 0
- head_gain: float32 [8, 64], P('tp'), may hold values from 0.1 to 1.9
- conv_taps: float32 [31, 1024], P(None, 'tp'), may hold values from -2.873685 to 2.873685
- channel_gain: float32 [1024], P('tp'), may hold values from 0.1 to 1.9
- channel_bias: float32 [1024], P('tp'), may hold values from -3 to 3
- w_out_attn: bfloat16 [512, 2048], P('tp'), may hold values from -0.15625 to 0.15625
- w_out_conv: bfloat16 [1024, 2048], P('tp'), may hold values from -0.15625 to 0.15625
- out_gain: float32 [2048], replicated, may hold values from 0.1 to 1.9
Outputs:
- mixed: bfloat16 [1024, 2048], P(('grp', 'sp')), parts along dimension 0
- log_mass: float32 [8, 1024], P('tp', ('grp', 'sp')), parts along dimension 1
There are 2 independent parts, one for each index of `grp`. A program takes and returns all parts, laid end to end along the dimension named above; an argument that names none is the same for every part. Nothing has to cross between parts.
All inputs are finite; a program needn't handle non-finite values.
Results may differ from a plain program's by a relative error of at most 0.011.
Values may be sent and summed in bfloat16 or wider, within the bound.
No kernel may reach another device: no remote copies, remote signals or barrier semaphores. Data moves between devices by JAX's collectives and lax.ppermute only.
A program may use at most 64 MiB of HBM per device.

v0:
```python
import jax
import jax.numpy as jnp
from jax import lax
from jax.sharding import PartitionSpec as P

HD = 64
CW = 1024
norm_eps = 1e-06


def from_behind(value, axis, steps):
    count = lax.axis_size(axis)
    initial, last = (max(0, -steps), min(count, count - steps))
    return lax.ppermute(value, axis, [(source, source + steps) for source in range(initial, last)])


def row_norm(values_in, gain_vec):
    squares = jnp.mean(values_in * values_in, axis=-1, keepdims=True)
    return values_in * lax.rsqrt(squares + norm_eps) * gain_vec


def local(
    tokens,
    norm_gain,
    w_query,
    w_key,
    w_value,
    w_glu_value,
    w_glu_gate,
    key_offset,
    head_gain,
    conv_taps,
    channel_gain,
    channel_bias,
    w_out_attn,
    w_out_conv,
    out_gain,
):
    row_count = tokens.shape[0]
    normed = row_norm(tokens.astype(jnp.float32), norm_gain).astype(jnp.bfloat16)
    weights_in = (w_query, w_key, w_value, w_glu_value, w_glu_gate)
    pieces = (
        lax.all_gather(weights_in[0], "sp", axis=0, tiled=True),
        lax.all_gather(weights_in[1], "sp", axis=0, tiled=True),
        lax.all_gather(weights_in[2], "sp", axis=0, tiled=True),
        lax.all_gather(weights_in[3], "sp", axis=0, tiled=True),
        lax.all_gather(weights_in[4], "sp", axis=0, tiled=True),
    )
    projected = tuple(
        (jnp.dot(normed, shard_piece, preferred_element_type=jnp.float32) for shard_piece in pieces)
    )
    query, key_rows, value_rows, glu_value, glu_gate = [
        summed.astype(jnp.bfloat16) for summed in projected
    ]
    kv_local = key_rows.shape[1] // HD
    group_size = query.shape[1] // key_rows.shape[1]
    heads_local = kv_local * group_size
    all_keys, all_values, all_offsets = (
        lax.all_gather(key_rows, "sp", axis=0, tiled=True),
        lax.all_gather(value_rows, "sp", axis=0, tiled=True),
        lax.all_gather(key_offset, "sp", axis=0, tiled=True),
    )
    sequence_length_total = all_keys.shape[0]
    shard_count = lax.axis_size("sp")
    per_block = 1
    while (
        per_block * 2 <= shard_count
        and shard_count % (per_block * 2) == 0
        and (per_block * 2 * row_count <= 1024)
    ):
        per_block = per_block * 2
    span_len = per_block * row_count
    query_heads = query.reshape(row_count, kv_local, group_size, HD)
    key_heads = all_keys.reshape(sequence_length_total, kv_local, HD)
    value_heads = all_values.reshape(sequence_length_total, kv_local, HD)
    my_index = lax.axis_index("sp")
    query_pos = my_index * row_count + jnp.arange(row_count, dtype=jnp.int32)
    last_block = my_index // per_block
    zeros_mix = jnp.zeros((kv_local, group_size, row_count, HD), jnp.float32)
    zeros_row = jnp.zeros((kv_local, group_size, row_count), jnp.float32)

    def sweep(turn_index, carry):
        head_mix, mass_sum, carried = carry
        first_key = (last_block - turn_index) * span_len
        key_block = lax.dynamic_slice_in_dim(key_heads, first_key, span_len, 0)
        value_block = lax.dynamic_slice_in_dim(value_heads, first_key, span_len, 0)
        offset_block = lax.dynamic_slice_in_dim(all_offsets, first_key, span_len, 0).astype(
            jnp.float32
        )
        offset_block = offset_block.T.reshape(kv_local, group_size, 1, span_len)
        scores = (
            jnp.einsum("qhgd,khd->hgqk", query_heads, key_block, preferred_element_type=jnp.float32)
            * HD ** (-0.5)
            + offset_block
        )
        key_pos = first_key + jnp.arange(span_len, dtype=jnp.int32)
        allowed = key_pos[None, :] <= query_pos[:, None]
        log_not = jnp.where(allowed, jax.nn.log_sigmoid(-scores), 0.0)
        later = lax.cumsum(log_not, axis=3, reverse=True) - log_not + carried[..., None]
        weights = jnp.where(allowed, jnp.exp(jax.nn.log_sigmoid(scores) + later), 0.0)
        head_mix = head_mix + jnp.einsum(
            "hgqk,khd->hgqd",
            weights.astype(jnp.bfloat16),
            value_block,
            preferred_element_type=jnp.float32,
        )
        return (head_mix, mass_sum + jnp.sum(weights, axis=3), carried + jnp.sum(log_not, axis=3))

    head_mix, mass_sum, leftover = lax.fori_loop(
        0, last_block + 1, sweep, (zeros_mix, zeros_row, zeros_row)
    )
    log_mass = jnp.log(mass_sum).reshape(heads_local, row_count)
    head_rows = head_mix.transpose(2, 0, 1, 3).reshape(row_count, heads_local, HD)
    attended = (
        row_norm(head_rows, head_gain).astype(jnp.bfloat16).reshape(row_count, heads_local * HD)
    )
    gated = (glu_value.astype(jnp.float32) * jax.nn.sigmoid(glu_gate.astype(jnp.float32))).astype(
        jnp.bfloat16
    )
    reach_len = conv_taps.shape[0] - 1
    before = from_behind(gated[row_count - reach_len :], "sp", 1)
    padded = jnp.concatenate([before, gated], axis=0).astype(jnp.float32)
    conv_out = jnp.zeros(gated.shape, jnp.float32)
    for tap_index in range(conv_taps.shape[0]):
        conv_out = conv_out + conv_taps[tap_index] * padded[tap_index : tap_index + row_count]
    total_sum, total_squares = lax.psum(
        (jnp.sum(conv_out, axis=1), jnp.sum(conv_out * conv_out, axis=1)), "tp"
    )
    chan_mean = (total_sum / CW)[:, None]
    spread = (total_squares / CW)[:, None] - chan_mean * chan_mean
    centered = conv_out - chan_mean
    channel_out = jax.nn.silu(
        centered * lax.rsqrt(spread + norm_eps) * channel_gain + channel_bias
    ).astype(jnp.bfloat16)
    share = lax.psum_scatter(
        jnp.dot(attended, w_out_attn, preferred_element_type=jnp.float32)
        + jnp.dot(channel_out, w_out_conv, preferred_element_type=jnp.float32),
        "tp",
        scatter_dimension=0,
        tiled=True,
    )
    mixed = lax.all_gather(row_norm(share, out_gain).astype(jnp.bfloat16), "tp", axis=0, tiled=True)
    return (mixed, log_mass)


def solution(mesh):
    in_specs = (
        P(("grp", "sp"), None),
        P(),
        P("sp", "tp"),
        P("sp", "tp"),
        P("sp", "tp"),
        P("sp", "tp"),
        P("sp", "tp"),
        P(("grp", "sp"), "tp"),
        P("tp", None),
        P(None, "tp"),
        P("tp"),
        P("tp"),
        P("tp", None),
        P("tp", None),
        P(),
    )
    out_specs = (P(("grp", "sp"), None), P("tp", ("grp", "sp")))
    return jax.shard_map(local, mesh=mesh, in_specs=in_specs, out_specs=out_specs, check_vma=False)
```

profile of v0, /device:TPU:0, one launch (start us, length us, event | category | flops | bytes accessed | tf_op | source)
XLA Modules:
  0.0 168.1 jit_solution(18097645065637768242)
XLA Ops:
  7.2 0.7 all-gather.3.cloned.1.call-update
  8.0 0.7 all-gather.5.cloned.1.call-update
  9.0 0.7 copy-done.4
  9.7 21.4 %all_gather.28 = bf16[2048,128]{1,0:T(8,128)(2,1)S(1)} all-gather(bf16[512,128]{1,0:T(8,128)(2,1)S(1)} %copy-done.4), channel_id=1, replica_groups=mesh['grp'=2,'sp'=4,'tp'=4] {'sp'}, dimensions={0}, use_global_device_ids=true | all-gather | bytes 655360 | tf_op jit(solution)/shard_map/all_gather | solution.py:44
  31.4 14.8 %all_gather.29 = bf16[512,128]{1,0:T(8,128)(2,1)S(1)} all-gather(bf16[128,128]{1,0:T(8,128)(2,1)S(1)} %convolution_convert_fusion.3), channel_id=1, replica_groups=mesh['grp'=2,'sp'=4,'tp'=4] {'sp'}, dimensions={0}, use_global_device_ids=true | all-gather | bytes 163840 | tf_op jit(solution)/shard_map/all_gather | solution.py:59
  46.4 0.8 copy-done.5
  47.2 18.3 %all_gather.31 = bf16[2048,128]{1,0:T(8,128)(2,1)S(1)} all-gather(bf16[512,128]{1,0:T(8,128)(2,1)S(1)} %copy-done.5), channel_id=1, replica_groups=mesh['grp'=2,'sp'=4,'tp'=4] {'sp'}, dimensions={0}, use_global_device_ids=true | all-gather | bytes 655360 | tf_op jit(solution)/shard_map/all_gather | solution.py:45
  65.8 15.0 %all_gather.32 = bf16[512,128]{1,0:T(8,128)(2,1)S(1)} all-gather(bf16[128,128]{1,0:T(8,128)(2,1)S(1)} %convolution_convert_fusion.2), channel_id=1, replica_groups=mesh['grp'=2,'sp'=4,'tp'=4] {'sp'}, dimensions={0}, use_global_device_ids=true | all-gather | bytes 163840 | tf_op jit(solution)/shard_map/all_gather | solution.py:60
  81.0 0.8 copy-done.6
  81.8 14.7 %all_gather.27 = bf16[2048,128]{1,0:T(8,128)(2,1)S(1)} all-gather(bf16[512,128]{1,0:T(8,128)(2,1)S(1)} %copy-done.6), channel_id=1, replica_groups=mesh['grp'=2,'sp'=4,'tp'=4] {'sp'}, dimensions={0}, use_global_device_ids=true | all-gather | bytes 655360 | tf_op jit(solution)/shard_map/all_gather | solution.py:43
  96.4 0.4 convolution_convert_fusion.4
  96.9 0.6 copy-done.11
  97.5 9.8 %all_gather.30 = bf16[512,2]{0,1:T(2,128)(2,1)S(1)} all-gather(bf16[128,2]{0,1:T(2,128)(2,1)S(1)} %copy-done.11), channel_id=1, replica_groups=mesh['grp'=2,'sp'=4,'tp'=4] {'sp'}, dimensions={0}, use_global_device_ids=true | all-gather | bytes 2560 | tf_op jit(solution)/shard_map/all_gather | solution.py:61
  107.3 4.3 %while.15 = (s32[]{:T(128)}, f32[2,1,128,64]{2,3,0,1:T(8,128)S(1)}, f32[2,1,128]{2,1,0:T(1,128)S(1)}, f32[2,1,128]{2,0,1:T(2,128)S(1)}, s32[]{:T(128)}, /*index=...) while((s32[]{:T(128)}, f32[2,1,128,64]{2,3,0,1:T(8,128)S(1)}, ...), condition=%wide.region_6.7_spmd.clone, body=%wide.region_1.6_spmd.clone.sunk | while | flops 54744452 | bytes 5395625 | solution.py:109
  107.4 0.6 fusion.104
  108.0 2.4 %fusion.105 = f32[2,1,128,4,128]{2,3,4,1,0:T(4,128)S(1)} fusion(f32[2,1,128,4,128]{2,4,3,0,1:T(8,128)S(1)} %bitcast.128), kind=kOutput, calls=%fused_computation.18.clone.1 | output fusion | flops 16646144 | bytes 1048576 | tf_op jit(solution)/shard_map/reduce-window
  110.5 0.8 fusion.106
  111.6 0.7 copy-done.7
  112.3 1.6 fusion.27
  114.0 1.6 fusion.26
  115.6 1.7 %collective-permute-start = (bf16[30,256]{1,0:T(8,128)(2,1)S(1)}, bf16[30,256]{1,0:T(8,128)(2,1)S(1)}, u32[]{:S(2)}, u32[]{:S(2)}) collective-permute-start(bf16[30,256]{1,0:T(8,128)(2,1)S(1)} %slice.262), channel_id=1, source_target_pairs={{0,4},{4,8},{8,12},{1,5},{5,9},{9,13},{2,6},{6,10},{10,14},{3,7},{... | collective-permute-start | bytes 46088 | tf_op jit(solution)/shard_map/ppermute | solution.py:14
  117.5 1.2 collective-permute-done
  118.8 0.6 fusion.76
  119.4 5.7 %all-reduce = (f32[128]{0:T(128)S(1)}, f32[128]{0:T(128)S(1)}) all-reduce(f32[128]{0:T(128)S(1)} %get-tuple-element.112, f32[128]{0:T(128)S(1)} %get-tuple-element.111), channel_id=1, replica_groups=mesh['grp'=2,'sp'=4,'tp'=4] {'tp'}, use_global_device_ids=true, to_apply=%region_11.12 | all-reduce | flops 256 | bytes 2048 | tf_op jit(solution)/shard_map/psum | solution.py:126
  125.0 0.7 copy-done.9
  126.1 0.7 copy-done.3
  126.8 1.3 convolution_add_fusion
  128.1 0.6 log_bitcast_fusion
  128.7 24.2 %reduce-scatter.2.cloned.1.call-done = f32[32,2048]{1,0:T(8,128)} async-done(((f32[128,2048]{1,0:T(8,128)}), f32[32,2048]{1,0:T(8,128)}) %reduce-scatter.2.cloned.1.call-update) | async-done | bytes 262160 | tf_op jit(solution)/shard_map/reduce_scatter | solution.py:135
  152.9 1.1 multiply_reduce_fusion
  154.1 6.6 %all_gather.35 = bf16[128,2048]{1,0:T(8,128)(2,1)S(1)} all-gather(bf16[32,2048]{1,0:T(8,128)(2,1)S(1)} %multiply_convert_fusion), channel_id=1, replica_groups=mesh['grp'=2,'sp'=4,'tp'=4] {'tp'}, dimensions={0}, use_global_device_ids=true | all-gather | bytes 655360 | tf_op jit(solution)/shard_map/all_gather | solution.py:142
  160.7 0.8 copy.53
  (59 shorter events, 2.5 us)
Async XLA Ops:
  7.2 117.9 %copy-start = (bf16[256,2048]{1,0:T(8,128)(2,1)S(1)}, bf16[256,2048]{1,0:T(8,128)(2,1)}, u32[]{:S(2)}) copy-start(bf16[256,2048]{1,0:T(8,128)(2,1)} %param.30) | copy-start | bytes 3145732
  7.2 1.6 copy-start.2
  7.2 105.2 %all-gather.3.cloned.1.call-start = ((), (), s32[]{:S(2)}) async-start(), calls=%async_computation.1 | async-start | bytes 1310720 | tf_op jit(solution)/shard_map/all_gather | solution.py:46
  7.9 106.0 %all-gather.5.cloned.1.call-start = ((), (), s32[]{:S(2)}) async-start(), calls=%async_computation.2 | async-start | bytes 1310720 | tf_op jit(solution)/shard_map/all_gather | solution.py:47
  8.7 144.2 %reduce-scatter.2.cloned.1.call-start = ((), (), s32[]{:S(2)}) async-start(), calls=%async_computation.3 | async-start | bytes 1310720 | tf_op jit(solution)/shard_map/reduce_scatter | solution.py:135
  8.7 0.9 copy-start.4
  9.7 21.4 %copy-start.12 = (f32[2048]{0:T(1024)S(1)}, f32[2048]{0:T(1024)}, u32[]{:S(2)}) copy-start(f32[2048]{0:T(1024)} %param.18) | copy-start | bytes 24580
  46.2 0.9 copy-start.5
  80.8 0.9 copy-start.6
  96.8 0.7 copy-start.11
  111.5 0.8 copy-start.7
  115.6 1.8 %copy-start.13 = (f32[2,64]{1,0:T(2,128)S(1)}, f32[2,64]{1,0:T(2,128)}, u32[]{:S(2)}) copy-start(f32[2,64]{1,0:T(2,128)} %param.25) | copy-start | bytes 1540
  115.6 3.2 %collective-permute-start = (bf16[30,256]{1,0:T(8,128)(2,1)S(1)}, bf16[30,256]{1,0:T(8,128)(2,1)S(1)}, u32[]{:S(2)}, u32[]{:S(2)}) collective-permute-start(bf16[30,256]{1,0:T(8,128)(2,1)S(1)} %slice.262), channel_id=1, source_target_pairs={{0,4},{4,8},{8,12},{1,5},{5,9},{9,13},{2,6},{6,10},{10,14},{3,7},{... | collective-permute-start | bytes 46088 | tf_op jit(solution)/shard_map/ppermute | solution.py:14
  118.8 6.3 %copy-start.10 = (f32[256]{0:T(256)S(1)}, f32[256]{0:T(256)}, u32[]{:S(2)}) copy-start(f32[256]{0:T(256)} %param.27) | copy-start | bytes 3076
  125.0 0.7 copy-start.9
  125.7 1.0 copy-start.3
  128.1 26.0 %copy-start.8 = (f32[2048]{0:T(1024)S(1)}, f32[2048]{0:T(1024)}, u32[]{:S(2)}) copy-start(f32[2048]{0:T(1024)} %param.31) | copy-start | bytes 24580
  152.9 1.2 copy-start.1
Sparse Core Ops, SparseCore 0:
  9.6 35.8 all-gather.2
  47.1 34.8 all-gather.4
  128.2 24.6 reduce-scatter.1
where the time goes:
time: 169 us; the launch traced here: 168 us
  blocking collectives  106 us (63%)
  waiting for transfers between devices  26.9 us (16%)
  between operations  14 us (8%)
  local copies, waits for them, and re-layouts  6.76 us (4%)
  matrix products  6.76 us (4%)
  other arithmetic  5.54 us (3%)
  starting transfers between devices  1.83 us (1%)
    reduce_scatter x1, waiting for transfers between devices, local(): lax.psum_scatter(jnp.dot(attended, w_out_attn, preferred_element_type=jnp...  24.2 us
    all_gather x1, blocking collectives, local(): lax.all_gather(weights_in[1], 'sp', axis=0, tiled=True)  21.4 us
    all_gather x1, blocking collectives, local(): lax.all_gather(weights_in[2], 'sp', axis=0, tiled=True)  18.3 us
    all_gather x1, blocking collectives, local(): lax.all_gather(value_rows, 'sp', axis=0, tiled=True)  15 us
    all_gather x1, blocking collectives, local(): lax.all_gather(key_rows, 'sp', axis=0, tiled=True)  14.8 us
    all_gather x1, blocking collectives, local(): lax.all_gather(weights_in[0], 'sp', axis=0, tiled=True)  14.7 us
    all_gather x1, blocking collectives, local(): lax.all_gather(key_offset, 'sp', axis=0, tiled=True)  9.75 us
    all_gather x1, blocking collectives, local(): lax.all_gather(row_norm(share, out_gain).astype(jnp.bfloat16), 'tp', axis...  6.6 us
  transfers between devices with their start and end apart: 4, of which 2 were waited for; matrix products, arithmetic and copies ran while one was open for 5% of the time, Pallas kernels for 0%

commit v1 on v0

--- a/solution.py
+++ b/solution.py
@@ -41,7 +41,9 @@
     weights_in = (w_query, w_key, w_value, w_glu_value, w_glu_gate)
     pieces = (
         lax.all_gather(weights_in[0], "sp", axis=0, tiled=True),
-        lax.all_gather(weights_in[1], "sp", axis=0, tiled=True),
+        jnp.concatenate(
+            lax.all_to_all(jnp.stack([weights_in[1]] * lax.axis_size("sp")), "sp", 0, 0), axis=0
+        ),
         lax.all_gather(weights_in[2], "sp", axis=0, tiled=True),
         lax.all_gather(weights_in[3], "sp", axis=0, tiled=True),
         lax.all_gather(weights_in[4], "sp", axis=0, tiled=True),

time: 169 us -> 177 us (1.047)
  starting transfers between devices: 1.83 us -> 7.85 us
  blocking collectives: 106 us -> 108 us
    all_gather x1 -> x0, blocking collectives: 21.4 us -> none  [local(): lax.all_gather(weights_in[1], 'sp', axis=0, tiled=True)]
    all_gather x1, blocking collectives: 18.3 us -> 39.7 us  [local(): lax.all_gather(weights_in[2], 'sp', axis=0, tiled=True)]
    all_to_all x0 -> x1, starting transfers between devices: none -> 6.48 us  [local(): lax.all_to_all(jnp.stack([weights_in[1]] * lax.axis_size('sp')), 'sp', 0, 0)]
    all_gather x1, blocking collectives: 14.7 us -> 18.7 us  [local(): lax.all_gather(weights_in[0], 'sp', axis=0, tiled=True)]
  transfers between devices with their start and end apart: 4 -> 5, of which waited for: 2 -> 2; matrix products, arithmetic and copies ran while one was open for 5% -> 5% of each run, Pallas kernels for 0% -> 0%
where the time goes in v1:
time: 177 us
  blocking collectives  108 us (61%)
  waiting for transfers between devices  27.3 us (15%)
  between operations  14 us (8%)
  starting transfers between devices  7.85 us (4%)
  matrix products  6.74 us (4%)
  local copies, waits for them, and re-layouts  6.68 us (4%)
  other arithmetic  5.53 us (3%)
    all_gather x1, blocking collectives, local(): lax.all_gather(weights_in[2], 'sp', axis=0, tiled=True)  39.7 us
    reduce_scatter x1, waiting for transfers between devices, local(): lax.psum_scatter(jnp.dot(attended, w_out_attn, preferred_element_type=jnp...  24.5 us
    all_gather x1, blocking collectives, local(): lax.all_gather(weights_in[0], 'sp', axis=0, tiled=True)  18.7 us
    all_gather x1, blocking collectives, local(): lax.all_gather(value_rows, 'sp', axis=0, tiled=True)  14.4 us
    all_gather x1, blocking collectives, local(): lax.all_gather(key_rows, 'sp', axis=0, tiled=True)  13.4 us
    all_gather x1, blocking collectives, local(): lax.all_gather(key_offset, 'sp', axis=0, tiled=True)  9.91 us
    all_gather x1, blocking collectives, local(): lax.all_gather(row_norm(share, out_gain).astype(jnp.bfloat16), 'tp', axis...  6.62 us
    all_to_all x1, starting transfers between devices, local(): lax.all_to_all(jnp.stack([weights_in[1]] * lax.axis_size('sp')), 'sp', 0, 0)  6.48 us
  transfers between devices with their start and end apart: 5, of which 2 were waited for; matrix products, arithmetic and copies ran while one was open for 5% of the time, Pallas kernels for 0%

profile of v1, /device:TPU:0, one launch (start us, length us, event | category | flops | bytes accessed | tf_op | source)
XLA Modules:
  0.0 176.6 jit_solution(10923173160230297773)
XLA Ops:
  7.2 0.7 all-gather.3.cloned.1.call-update
  8.2 0.9 stack.2
  9.0 6.5 %all-to-all-start = ((bf16[4,512,128]{2,1,0:T(8,128)(2,1)}), bf16[4,512,128]{2,1,0:T(8,128)(2,1)S(1)}, u32[]{:S(2)}, u32[]{:S(2)}) async-start(bf16[4,512,128]{2,1,0:T(8,128)(2,1)} %stack.2), calls=%async_computation | async-start | bytes 1048576 | tf_op jit(solution)/shard_map/all_to_all | solution.py:45
  15.5 0.7 all-gather.5.cloned.1.call-update
  16.5 0.6 copy-done.5
  17.2 39.7 %all_gather.27 = bf16[2048,128]{1,0:T(8,128)(2,1)S(1)} all-gather(bf16[512,128]{1,0:T(8,128)(2,1)S(1)} %copy-done.5), channel_id=1, replica_groups=mesh['grp'=2,'sp'=4,'tp'=4] {'sp'}, dimensions={0}, use_global_device_ids=true | all-gather | bytes 655360 | tf_op jit(solution)/shard_map/all_gather | solution.py:47
  57.2 0.5 copy-done.6
  57.7 18.7 %all_gather.24 = bf16[2048,128]{1,0:T(8,128)(2,1)S(1)} all-gather(bf16[512,128]{1,0:T(8,128)(2,1)S(1)} %copy-done.6), channel_id=1, replica_groups=mesh['grp'=2,'sp'=4,'tp'=4] {'sp'}, dimensions={0}, use_global_device_ids=true | all-gather | bytes 655360 | tf_op jit(solution)/shard_map/all_gather | solution.py:43
  76.4 14.4 %all_gather.28 = bf16[512,128]{1,0:T(8,128)(2,1)S(1)} all-gather(bf16[128,128]{1,0:T(8,128)(2,1)S(1)} %convolution_convert_fusion.2), channel_id=1, replica_groups=mesh['grp'=2,'sp'=4,'tp'=4] {'sp'}, dimensions={0}, use_global_device_ids=true | all-gather | bytes 163840 | tf_op jit(solution)/shard_map/all_gather | solution.py:62
  91.0 0.7 copy-done.13
  91.7 0.6 copy-done.11
  92.3 9.9 %all_gather.26 = bf16[512,2]{0,1:T(2,128)(2,1)S(1)} all-gather(bf16[128,2]{0,1:T(2,128)(2,1)S(1)} %copy-done.11), channel_id=1, replica_groups=mesh['grp'=2,'sp'=4,'tp'=4] {'sp'}, dimensions={0}, use_global_device_ids=true | all-gather | bytes 2560 | tf_op jit(solution)/shard_map/all_gather | solution.py:63
  102.2 0.4 convolution_convert_fusion.4
  103.0 13.4 %all_gather.25 = bf16[512,128]{1,0:T(8,128)(2,1)S(1)} all-gather(bf16[128,128]{1,0:T(8,128)(2,1)S(1)} %convolution_convert_fusion.3), channel_id=1, replica_groups=mesh['grp'=2,'sp'=4,'tp'=4] {'sp'}, dimensions={0}, use_global_device_ids=true | all-gather | bytes 163840 | tf_op jit(solution)/shard_map/all_gather | solution.py:61
  116.6 4.3 %while.15 = (s32[]{:T(128)}, f32[2,1,128,64]{2,3,0,1:T(8,128)S(1)}, f32[2,1,128]{2,1,0:T(1,128)S(1)}, f32[2,1,128]{2,0,1:T(2,128)S(1)}, s32[]{:T(128)}, /*index=...) while((s32[]{:T(128)}, f32[2,1,128,64]{2,3,0,1:T(8,128)S(1)}, ...), condition=%wide.region_6.7_spmd.clone, body=%wide.region_1.6_spmd.clone.sunk | while | flops 54744452 | bytes 5395625 | solution.py:111
  116.8 0.6 fusion.104
  117.4 2.4 %fusion.105 = f32[2,1,128,4,128]{2,3,4,1,0:T(4,128)S(1)} fusion(f32[2,1,128,4,128]{2,4,3,0,1:T(8,128)S(1)} %bitcast.129), kind=kOutput, calls=%fused_computation.18.clone.1 | output fusion | flops 16646144 | bytes 1048576 | tf_op jit(solution)/shard_map/reduce-window
  119.8 0.8 fusion.106
  120.9 1.6 fusion.27
  122.5 1.6 fusion.26
  124.2 1.3 collective-permute-start
  125.6 1.3 collective-permute-done
  126.9 0.6 fusion.76
  127.5 5.8 %all-reduce = (f32[128]{0:T(128)S(1)}, f32[128]{0:T(128)S(1)}) all-reduce(f32[128]{0:T(128)S(1)} %get-tuple-element.112, f32[128]{0:T(128)S(1)} %get-tuple-element.111), channel_id=1, replica_groups=mesh['grp'=2,'sp'=4,'tp'=4] {'tp'}, use_global_device_ids=true, to_apply=%region_11.12 | all-reduce | flops 256 | bytes 2048 | tf_op jit(solution)/shard_map/psum | solution.py:128
  133.3 0.7 copy-done.9
  134.3 0.7 copy-done.3
  135.0 1.3 convolution_add_fusion
  136.3 0.6 log_bitcast_fusion
  136.9 24.5 %reduce-scatter.2.cloned.1.call-done = f32[32,2048]{1,0:T(8,128)} async-done(((f32[128,2048]{1,0:T(8,128)}), f32[32,2048]{1,0:T(8,128)}) %reduce-scatter.2.cloned.1.call-update) | async-done | bytes 262160 | tf_op jit(solution)/shard_map/reduce_scatter | solution.py:137
  161.4 1.1 multiply_reduce_fusion
  162.6 6.6 %all_gather.31 = bf16[128,2048]{1,0:T(8,128)(2,1)S(1)} all-gather(bf16[32,2048]{1,0:T(8,128)(2,1)S(1)} %multiply_convert_fusion), channel_id=1, replica_groups=mesh['grp'=2,'sp'=4,'tp'=4] {'tp'}, dimensions={0}, use_global_device_ids=true | all-gather | bytes 655360 | tf_op jit(solution)/shard_map/all_gather | solution.py:144
  169.3 0.8 copy.53
  (61 shorter events, 2.8 us)
Async XLA Ops:
  7.2 126.1 %copy-start = (bf16[256,2048]{1,0:T(8,128)(2,1)S(1)}, bf16[256,2048]{1,0:T(8,128)(2,1)}, u32[]{:S(2)}) copy-start(bf16[256,2048]{1,0:T(8,128)(2,1)} %param.30) | copy-start | bytes 3145732
  7.2 1.0 copy-start.4
  7.2 113.7 %all-gather.3.cloned.1.call-start = ((), (), s32[]{:S(2)}) async-start(), calls=%async_computation.2 | async-start | bytes 1310720 | tf_op jit(solution)/shard_map/all_gather | solution.py:48
  9.0 7.3 %copy-start.2 = (bf16[128,2048]{1,0:T(8,128)(2,1)S(1)}, bf16[128,2048]{1,0:T(8,128)(2,1)}, u32[]{:S(2)}) copy-start(bf16[128,2048]{1,0:T(8,128)(2,1)} %param.17) | copy-start | bytes 1572868
  9.0 93.6 %all-to-all-start = ((bf16[4,512,128]{2,1,0:T(8,128)(2,1)}), bf16[4,512,128]{2,1,0:T(8,128)(2,1)S(1)}, u32[]{:S(2)}, u32[]{:S(2)}) async-start(bf16[4,512,128]{2,1,0:T(8,128)(2,1)} %stack.2), calls=%async_computation | async-start | bytes 1048576 | tf_op jit(solution)/shard_map/all_to_all | solution.py:45
  15.5 107.0 %all-gather.5.cloned.1.call-start = ((), (), s32[]{:S(2)}) async-start(), calls=%async_computation.3 | async-start | bytes 1310720 | tf_op jit(solution)/shard_map/all_gather | solution.py:49
  16.2 0.9 copy-start.5
  16.3 145.1 %reduce-scatter.2.cloned.1.call-start = ((), (), s32[]{:S(2)}) async-start(), calls=%async_computation.4 | async-start | bytes 1310720 | tf_op jit(solution)/shard_map/reduce_scatter | solution.py:137
  17.2 39.7 %copy-start.12 = (f32[2048]{0:T(1024)S(1)}, f32[2048]{0:T(1024)}, u32[]{:S(2)}) copy-start(f32[2048]{0:T(1024)} %param.18) | copy-start | bytes 24580
  56.8 0.9 copy-start.6
  90.8 11.4 %copy-start.7 = (f32[31,256]{1,0:T(8,128)S(1)}, f32[31,256]{1,0:T(8,128)}, u32[]{:S(2)}) copy-start(f32[31,256]{1,0:T(8,128)} %param.26) | copy-start | bytes 95236
  90.9 0.7 copy-start.13
  91.6 0.7 copy-start.11
  124.2 2.7 %collective-permute-start = (bf16[30,256]{1,0:T(8,128)(2,1)S(1)}, bf16[30,256]{1,0:T(8,128)(2,1)S(1)}, u32[]{:S(2)}, u32[]{:S(2)}) collective-permute-start(bf16[30,256]{1,0:T(8,128)(2,1)S(1)} %slice.262), channel_id=1, source_target_pairs={{0,4},{4,8},{8,12},{1,5},{5,9},{9,13},{2,6},{6,10},{10,14},{3,7},{... | collective-permute-start | bytes 46088 | tf_op jit(solution)/shard_map/ppermute | solution.py:14
  126.9 6.4 %copy-start.10 = (f32[256]{0:T(256)S(1)}, f32[256]{0:T(256)}, u32[]{:S(2)}) copy-start(f32[256]{0:T(256)} %param.27) | copy-start | bytes 3076
  133.3 0.7 copy-start.9
  133.9 1.0 copy-start.3
  136.3 26.2 %copy-start.8 = (f32[2048]{0:T(1024)S(1)}, f32[2048]{0:T(1024)}, u32[]{:S(2)}) copy-start(f32[2048]{0:T(1024)} %param.31) | copy-start | bytes 24580
  161.4 1.2 copy-start.1
Sparse Core Ops, SparseCore 0:
  9.6 45.3 all-gather.2
  56.6 31.2 all-gather.4
  136.4 24.8 reduce-scatter.1
